TPU v7x, 512 devices: a 4x2x32 block of a 4x8x32 slice. The times are simulated.
512 devices in a mesh: grp: 2 (over y), sp: 32 (over z), tp: 8 (over x, core).
Axes of the slice: x: 4, y: 2, z: 32, core: 2. Of those that a mesh axis runs over, the one named last changes fastest.
The devices are a block of a 4x8x32 slice.
Arguments:
- inputs: bfloat16 [16384, 2048], P(('grp', 'sp'), 'tp'), parts along dimension 0, may hold values from -20 to 20
- norm_gain: bfloat16 [2048], replicated, may hold values from 0.099609375 to 1.8984375
- w_conv_in: bfloat16 [1024, 2048], P('tp'), may hold values from -0.125 to 0.125
- w_conv_gate: bfloat16 [1024, 2048], P('tp'), may hold values from -0.125 to 0.125
- conv_kernel: bfloat16 [31, 1024], P(None, 'tp'), may hold values from -4.3105272 to 4.3105272
- ln_gain: bfloat16 [1024], P('tp'), may hold values from 0.099609375 to 1.8984375
- w_query: bfloat16 [1024, 2048], P('tp'), may hold values from -0.53033009 to 0.53033009
- w_key: bfloat16 [1024, 2048], P('tp'), may hold values from -0.53033009 to 0.53033009
- w_value: bfloat16 [1024, 2048], P('tp'), may hold values from -0.125 to 0.125
- cum_gate: float32 [16, 16384], P('tp', ('grp', 'sp')), parts along dimension 1, may hold values from -8192 to 0, as said below
- w_conv_out: bfloat16 [1024, 2048], P('tp'), may hold values from -0.125 to 0.125
- w_attn_out: bfloat16 [1024, 2048], P('tp'), may hold values from -0.125 to 0.125
Outputs:
- mixed: bfloat16 [16384, 2048], P(('grp', 'sp', 'tp')), parts along dimension 0
- log_total: float32 [16, 16384], P('tp', ('grp', 'sp')), parts along dimension 1
There are 2 independent parts, one for each index of `grp`. A program takes and returns all parts, laid end to end along the dimension named above; an argument that names none is the same for every part. Nothing has to cross between parts.
Inputs may be any that keep to these rules, and one draw needn't show every extreme that they name: cum_gate never rises along positions: entry t is the sum of the head's log forget gates at positions 0 to t.
All inputs are finite; a program needn't handle non-finite values.
Results may differ from a plain program's by a relative error of at most 0.0144.
Values may be sent and summed in bfloat16 or wider, within the bound.
A program may use at most 64 MiB of HBM per device.

v0:
```python
import jax
import jax.numpy as jnp
from jax import lax
from jax.sharding import PartitionSpec as P

D = 2048
CONV_CH = 1024
neg_large = -1e30


def sent_to_all(shard, axis):
    devices = lax.axis_size(axis)
    return lax.all_to_all(
        jnp.broadcast_to(shard[None], (devices, *shard.shape)), axis, 0, 0, tiled=True
    )


def in_order(parts, dim):
    lengths = list(parts.shape[1:])
    lengths[dim] *= parts.shape[0]
    return jnp.moveaxis(parts, 0, dim).reshape(lengths)


def gather_directly(shard, axis, dim):
    parts = sent_to_all(shard, axis)
    return in_order(parts, dim)


def passed_along(block, axis, distance):
    devices = range(lax.axis_size(axis))
    route = [(i - distance, i) for i in devices if i - distance in devices]
    return lax.ppermute(block, axis, route)


def sent_together(arrays, axis, dim, along):
    both = jnp.concatenate(arrays, axis=along)
    filled, at, outs = (lax.all_gather(both, axis, axis=dim, tiled=True), 0, [])
    for a in arrays:
        outs.append(lax.slice_in_dim(filled, at, at + a.shape[along], axis=along))
        at += a.shape[along]
    return tuple(outs)


def in_blocks(shard, dim, devices):
    lengths = shard.shape
    parts = shard.reshape(*lengths[:dim], devices, lengths[dim] // devices, *lengths[dim + 1 :])
    return jnp.moveaxis(parts, dim, 0)


def summed_on_arrival(shard, axis, dim):
    devices = lax.axis_size(axis)
    parts = lax.all_to_all(in_blocks(shard, dim, devices), axis, 0, 0, tiled=True)
    return jnp.sum(parts.astype(jnp.float32), axis=0)


def block_terms(q_blk, q_cum, k_blk, v_blk, k_cum, q_first, k_first):
    score_scale = q_blk.shape[2] ** (-0.5)
    scores = (
        jnp.einsum("qhd,khd->hqk", q_blk, k_blk, preferred_element_type=jnp.float32) * score_scale
    )
    scores = scores + q_cum[:, :, None] - k_cum[:, None, :]
    q_pos = q_first + jnp.arange(q_blk.shape[0], dtype=jnp.int32)
    k_pos = k_first + jnp.arange(k_blk.shape[0], dtype=jnp.int32)
    allowed = k_pos[None, :] <= q_pos[:, None]
    scores = jnp.where(allowed[None], scores, -jnp.inf)
    block_top = jnp.max(scores, axis=-1)
    weights = jnp.exp(scores - block_top[..., None])
    block_total = jnp.sum(weights, axis=-1)
    block_out = jnp.einsum(
        "hqk,khd->hqd", weights.astype(jnp.bfloat16), v_blk, preferred_element_type=jnp.float32
    ).astype(jnp.bfloat16)
    return (block_top, block_total, block_out)


def merge_terms(state, terms):
    top_now, total_now, acc_now = state
    block_top, block_total, block_out = terms
    top_new = jnp.maximum(top_now, block_top)
    keep_old = jnp.exp(top_now - top_new)
    keep_new = jnp.exp(block_top - top_new)
    return (
        top_new,
        total_now * keep_old + block_total * keep_new,
        acc_now * keep_old[..., None] + block_out.astype(jnp.float32) * keep_new[..., None],
    )


def local(
    inputs,
    norm_gain,
    w_conv_in,
    w_conv_gate,
    conv_kernel,
    ln_gain,
    w_query,
    w_key,
    w_value,
    cum_gate,
    w_conv_out,
    w_attn_out,
):
    rows_here = inputs.shape[0]
    conv_width = w_conv_in.shape[0]
    attn_width = w_query.shape[0]
    heads_here = cum_gate.shape[0]
    head_dim = attn_width // heads_here
    taps_count = conv_kernel.shape[0]
    w_all = jnp.concatenate([w_conv_in, w_conv_gate, w_query, w_key, w_value], axis=0)
    gain_all = norm_gain.astype(jnp.float32)
    contract_dims = (((1,), (1,)), ((), ()))
    piece_f = gather_directly(inputs, "tp", 1).astype(jnp.float32)
    scaled_piece = (piece_f * gain_all[None, :]).astype(jnp.bfloat16)
    raw_proj = lax.dot_general(
        scaled_piece, w_all, contract_dims, preferred_element_type=jnp.float32
    )
    squares = jnp.sum(piece_f * piece_f, axis=1)
    rms = lax.rsqrt(squares / D + 1e-06)[:, None]
    proj = raw_proj * rms
    conv_in = proj[:, :conv_width]
    conv_gate = proj[:, conv_width : 2 * conv_width]
    query = proj[:, 2 * conv_width : 2 * conv_width + attn_width].astype(jnp.bfloat16)
    key_rows = proj[:, 2 * conv_width + attn_width : 2 * conv_width + 2 * attn_width].astype(
        jnp.bfloat16
    )
    value = proj[:, 2 * conv_width + 2 * attn_width :].astype(jnp.bfloat16)
    glu = (conv_in * jax.nn.sigmoid(conv_gate)).astype(jnp.bfloat16)
    rim_rows = passed_along(glu[rows_here - (taps_count - 1) :], "sp", 1)
    extended = jnp.concatenate([rim_rows, glu], axis=0)
    kernel = conv_kernel.astype(jnp.float32)
    conv_sum = jnp.zeros((rows_here, conv_width), jnp.float32)
    for tap_idx in range(taps_count):
        conv_sum = (
            conv_sum
            + extended[tap_idx : tap_idx + rows_here].astype(jnp.float32) * kernel[tap_idx][None, :]
        )
    chan_first, chan_second = lax.psum(
        (jnp.sum(conv_sum, axis=1), jnp.sum(conv_sum * conv_sum, axis=1)), "tp"
    )
    chan_mean = (chan_first / CONV_CH)[:, None]
    chan_var = (chan_second / CONV_CH)[:, None] - chan_mean * chan_mean
    normed = (
        (conv_sum - chan_mean) * lax.rsqrt(chan_var + 1e-05) * ln_gain.astype(jnp.float32)[None, :]
    )
    conv_out = jax.nn.silu(normed).astype(jnp.bfloat16)
    q_heads = query.reshape(rows_here, heads_here, head_dim)
    cum_all = lax.all_gather(cum_gate.T, "sp", axis=0, tiled=True)
    own_first = lax.axis_index("sp") * rows_here
    start_state = (
        jnp.full((heads_here, rows_here), neg_large, jnp.float32),
        jnp.zeros((heads_here, rows_here), jnp.float32),
        jnp.zeros((heads_here, rows_here, head_dim), jnp.float32),
    )
    state = start_state
    k_piece, v_piece = sent_together((key_rows, value), "sp", 0, 1)
    block_count = k_piece.shape[0] // rows_here
    k_split = k_piece.reshape(block_count, rows_here, heads_here, head_dim)
    v_split = v_piece.reshape(block_count, rows_here, heads_here, head_dim)

    def visit(carry, item):
        k_blk, v_blk, block_idx = item
        k_first = block_idx * rows_here
        k_cum = lax.dynamic_slice_in_dim(cum_all, k_first, rows_here, 0).T

        def take_block(inner):
            return merge_terms(
                inner, block_terms(q_heads, cum_gate, k_blk, v_blk, k_cum, own_first, k_first)
            )

        def skip_block(inner):
            return inner

        return (lax.cond(k_first <= own_first, take_block, skip_block, carry), None)

    state, unused = lax.scan(
        visit, state, (k_split, v_split, jnp.arange(block_count, dtype=jnp.int32))
    )
    top_all, total_all, acc_all = state
    attn_out = (
        (acc_all / total_all[..., None])
        .transpose(1, 0, 2)
        .reshape(rows_here, attn_width)
        .astype(jnp.bfloat16)
    )
    log_total = top_all + jnp.log(total_all)
    mixed = summed_on_arrival(
        (
            jnp.dot(conv_out, w_conv_out, preferred_element_type=jnp.float32)
            + jnp.dot(attn_out, w_attn_out, preferred_element_type=jnp.float32)
        ).astype(jnp.bfloat16),
        "tp",
        0,
    ).astype(jnp.bfloat16)
    return (mixed, log_total)


def solution(mesh):
    in_specs = (
        P(("grp", "sp"), "tp"),
        P(),
        P("tp", None),
        P("tp", None),
        P(None, "tp"),
        P("tp"),
        P("tp", None),
        P("tp", None),
        P("tp", None),
        P("tp", ("grp", "sp")),
        P("tp", None),
        P("tp", None),
    )
    out_specs = (P(("grp", "sp", "tp"), None), P("tp", ("grp", "sp")))
    return jax.shard_map(local, mesh=mesh, in_specs=in_specs, out_specs=out_specs, check_vma=False)
```

profile of v0, /device:TPU:2016, one launch (start us, length us, event | category | flops | bytes accessed | tf_op | source)
XLA Modules:
  0.0 345.3 jit_solution(744768911133563822)
XLA Ops:
  9.4 4.6 %all-to-all-start = ((bf16[8,256,256]{1,2,0:T(8,128)(2,1)}), bf16[8,256,256]{1,2,0:T(8,128)(2,1)S(1)}, u32[]{:S(2)}, u32[]{:S(2)}) async-start(bf16[8,256,256]{1,2,0:T(8,128)(2,1)} %broadcast_in_dim.25), calls=%async_computation | async-start | bytes 2097152 | tf_op jit(solution)/shard_map/all_to_all | solution.py:13
  18.3 11.6 %all-to-all-done = bf16[8,256,256]{1,2,0:T(8,128)(2,1)S(1)} async-done(((bf16[8,256,256]{1,2,0:T(8,128)(2,1)}), bf16[8,256,256]{1,2,0:T(8,128)(2,1)S(1)}, u32[]{:S(2)}, u32[]{:S(2)}) %all-to-all-start) | async-done | bytes 1048608 | tf_op jit(solution)/shard_map/all_to_all | solution.py:13
  30.6 2.8 fusion.62
  35.6 53.0 %all_gather.6 = f32[8192,2]{0,1:T(2,128)S(1)} all-gather(f32[256,2]{0,1:T(2,128)S(1)} %bitcast.102), channel_id=1, replica_groups=mesh['grp'=2,'sp'=32,'tp'=8] {'sp'}, dimensions={0}, use_global_device_ids=true | all-gather | bytes 67584 | tf_op jit(solution)/shard_map/all_gather | solution.py:146
  89.5 12.5 %all-reduce = (f32[256]{0:T(256)S(1)}, f32[256]{0:T(256)S(1)}) all-reduce(f32[256]{0:T(256)S(1)} %get-tuple-element.184, f32[256]{0:T(256)S(1)} %get-tuple-element.183), channel_id=1, replica_groups=mesh['grp'=2,'sp'=32,'tp'=8] {'tp'}, use_global_device_ids=true, to_apply=%region_4.0 | all-reduce | flops 512 | bytes 4096 | tf_op jit(solution)/shard_map/psum | solution.py:136
  102.5 53.7 %all-gather.2.cloned.1.call-done = bf16[8192,256]{1,0:T(8,128)(2,1)} async-done(((bf16[256,256]{1,0:T(8,128)(2,1)}), bf16[8192,256]{1,0:T(8,128)(2,1)}) %all-gather.2.cloned.1.call-update) | async-done | bytes 4194320 | tf_op jit(solution)/shard_map/all_gather | solution.py:37
  156.1 4.5 %fusion.61 = (bf16[8192,128]{1,0:T(8,128)(2,1)}, bf16[8192,128]{1,0:T(8,128)(2,1)}) fusion(bf16[8192,256]{1,0:T(8,128)(2,1)} %all-gather.2.cloned.1.call-done), kind=kLoop, calls=%fused_computation.157 | loop fusion | bytes 8388608 | tf_op jit(solution)/shard_map/slice | solution.py:39
  160.6 8.2 %reshape.86 = bf16[32,256,2,64]{3,2,1,0:T(2,128)(2,1)} reshape(bf16[8192,128]{1,0:T(8,128)(2,1)} %get-tuple-element.218) | data formatting | bytes 4194304 | tf_op jit(solution)/shard_map/reshape | solution.py:157
  168.8 9.7 %copy.24 = bf16[32,256,2,64]{1,3,2,0:T(8,128)(2,1)} copy(bf16[32,256,2,64]{3,2,1,0:T(2,128)(2,1)} %reshape.86) | data formatting | bytes 4194304 | tf_op jit(solution)/shard_map/while | solution.py:174
  178.5 8.2 %reshape.85 = bf16[32,256,2,64]{3,2,1,0:T(2,128)(2,1)} reshape(bf16[8192,128]{1,0:T(8,128)(2,1)} %get-tuple-element.219) | data formatting | bytes 4194304 | tf_op jit(solution)/shard_map/reshape | solution.py:156
  186.7 9.8 %copy.23 = bf16[32,256,2,64]{1,3,2,0:T(8,128)(2,1)} copy(bf16[32,256,2,64]{3,2,1,0:T(2,128)(2,1)} %reshape.85) | data formatting | bytes 4194304 | tf_op jit(solution)/shard_map/while | solution.py:174
  196.5 119.1 %while.14 = (s32[]{:T(128)}, f32[2,256]{1,0:T(2,128)S(1)}, f32[2,256]{1,0:T(2,128)S(1)}, f32[2,256,64]{1,2,0:T(8,128)S(1)}, s32[32]{0:T(128)S(1)}, /*index=5*/s3...) while((s32[]{:T(128)}, f32[2,256]{1,0:T(2,128)S(1)}, ...), condition=%wide.region_10.11_spmd, body=%wide.region_5.10_spmd.sunk | while | flops 34966024 | bytes 2205049 | solution.py:174
  197.7 2.5 conditional.2
  201.4 2.5 conditional.2
  205.2 2.5 conditional.2
  216.3 2.5 conditional.2
  220.1 2.5 conditional.2
  227.5 2.5 conditional.2
  231.2 2.5 conditional.2
  242.4 2.5 conditional.2
  246.1 2.5 conditional.2
  257.3 2.5 conditional.2
  317.1 4.5 %all-to-all-start.1 = ((bf16[8,32,2048]{2,1,0:T(8,128)(2,1)}), bf16[8,32,2048]{2,1,0:T(8,128)(2,1)S(1)}, u32[]{:S(2)}, u32[]{:S(2)}) async-start(bf16[8,32,2048]{2,1,0:T(8,128)(2,1)} %bitcast.99), calls=%async_computation.1 | async-start | bytes 2097152 | tf_op jit(solution)/shard_map/all_to_all | solution.py:52
  322.3 15.3 %all-to-all-done.1 = bf16[8,32,2048]{2,1,0:T(8,128)(2,1)S(1)} async-done(((bf16[8,32,2048]{2,1,0:T(8,128)(2,1)}), bf16[8,32,2048]{2,1,0:T(8,128)(2,1)S(1)}, u32[]{:S(2)}, u32[]{:S(2)}) %all-to-all-start.1) | async-done | bytes 1048608 | tf_op jit(solution)/shard_map/all_to_all | solution.py:52
  (335 shorter events, 166.8 us)
Async XLA Ops:
  7.2 94.8 %copy-start = (bf16[128,2048]{1,0:T(8,128)(2,1)S(1)}, bf16[128,2048]{1,0:T(8,128)(2,1)}, u32[]{:S(2)}) copy-start(bf16[128,2048]{1,0:T(8,128)(2,1)} %param.26) | copy-start | bytes 1572868
  7.2 6.9 %copy-start.8 = (bf16[2048]{0:T(1024)(128)(2,1)S(1)}, bf16[2048]{0:T(1024)(128)(2,1)}, u32[]{:S(2)}) copy-start(bf16[2048]{0:T(1024)(128)(2,1)} %param.17) | copy-start | bytes 12292
  7.2 6.9 %copy-start.2 = (bf16[128,2048]{1,0:T(8,128)(2,1)S(1)}, bf16[128,2048]{1,0:T(8,128)(2,1)}, u32[]{:S(2)}) copy-start(bf16[128,2048]{1,0:T(8,128)(2,1)} %param.18) | copy-start | bytes 1572868
  7.2 7.7 %copy-start.3 = (bf16[128,2048]{1,0:T(8,128)(2,1)S(1)}, bf16[128,2048]{1,0:T(8,128)(2,1)}, u32[]{:S(2)}) copy-start(bf16[128,2048]{1,0:T(8,128)(2,1)} %param.19) | copy-start | bytes 1572868
  8.3 7.5 %copy-start.4 = (bf16[128,2048]{1,0:T(8,128)(2,1)S(1)}, bf16[128,2048]{1,0:T(8,128)(2,1)}, u32[]{:S(2)}) copy-start(bf16[128,2048]{1,0:T(8,128)(2,1)} %param.22) | copy-start | bytes 1572868
  9.4 20.5 %all-to-all-start = ((bf16[8,256,256]{1,2,0:T(8,128)(2,1)}), bf16[8,256,256]{1,2,0:T(8,128)(2,1)S(1)}, u32[]{:S(2)}, u32[]{:S(2)}) async-start(bf16[8,256,256]{1,2,0:T(8,128)(2,1)} %broadcast_in_dim.25), calls=%async_computation | async-start | bytes 2097152 | tf_op jit(solution)/shard_map/all_to_all | solution.py:13
  14.0 142.1 %all-gather.2.cloned.1.call-start = ((), (), s32[]{:S(2)}) async-start(), calls=%async_computation.2 | async-start | bytes 4325376 | tf_op jit(solution)/shard_map/all_gather | solution.py:37
  14.1 2.6 copy-start.5
  14.1 3.4 copy-start.6
  30.6 3.6 %copy-start.7 = (bf16[31,128]{1,0:T(8,128)(2,1)S(1)}, bf16[31,128]{1,0:T(8,128)(2,1)}, u32[]{:S(2)}) copy-start(bf16[31,128]{1,0:T(8,128)(2,1)} %param.20) | copy-start | bytes 23812
  30.6 5.0 %copy-start.9 = (f32[2,256]{1,0:T(2,128)S(1)}, f32[2,256]{1,0:T(2,128)}, u32[]{:S(2)}) copy-start(f32[2,256]{1,0:T(2,128)} %param.25) | copy-start | bytes 6148
  30.6 58.0 %copy-start.10 = (bf16[128]{0:T(256)(128)(2,1)S(1)}, bf16[128]{0:T(256)(128)(2,1)}, u32[]{:S(2)}) copy-start(bf16[128]{0:T(256)(128)(2,1)} %param.21) | copy-start | bytes 772
  34.3 54.5 %collective-permute-start = (bf16[30,128]{1,0:T(8,128)(2,1)S(1)}, bf16[30,128]{1,0:T(8,128)(2,1)S(1)}, u32[]{:S(2)}, u32[]{:S(2)}) collective-permute-start(bf16[30,128]{1,0:T(8,128)(2,1)S(1)} %slice.282), channel_id=1, source_target_pairs={{0,8},{8,16},{16,24},{24,32},{32,40},{40,48},{48,56},{56,64},{64,7... | collective-permute-start | bytes 23048 | tf_op jit(solution)/shard_map/ppermute | solution.py:32
  196.5 119.2 %copy-start.1 = (bf16[128,2048]{1,0:T(8,128)(2,1)S(1)}, bf16[128,2048]{1,0:T(8,128)(2,1)}, u32[]{:S(2)}) copy-start(bf16[128,2048]{1,0:T(8,128)(2,1)} %param.27) | copy-start | bytes 1572868
  317.1 20.5 %all-to-all-start.1 = ((bf16[8,32,2048]{2,1,0:T(8,128)(2,1)}), bf16[8,32,2048]{2,1,0:T(8,128)(2,1)S(1)}, u32[]{:S(2)}, u32[]{:S(2)}) async-start(bf16[8,32,2048]{2,1,0:T(8,128)(2,1)} %bitcast.99), calls=%async_computation.1 | async-start | bytes 2097152 | tf_op jit(solution)/shard_map/all_to_all | solution.py:52
Sparse Core Ops, SparseCore 0:
  34.3 121.7 all-gather.1
where the time goes:
time: 349 us; the launch traced here: 345 us
  waiting for transfers between devices  80.7 us (23%)
  matrix products  76.5 us (22%)
  local copies, waits for them, and re-layouts  66.7 us (19%)
  blocking collectives  65.5 us (19%)
  loops' own time  21.1 us (6%)
  between operations  14.3 us (4%)
  starting transfers between devices  10.5 us (3%)
  other arithmetic  10 us (3%)
    all_gather x1, waiting for transfers between devices, sent_together(): filled, at, outs = (lax.all_gather(both, axis, axis=dim, tiled=True), 0, [])  53.7 us
    all_gather x1, blocking collectives, local(): cum_all = lax.all_gather(cum_gate.T, 'sp', axis=0, tiled=True)  53 us
    dot_general x32, matrix products, block_terms(): jnp.einsum('qhd,khd->hqk', q_blk, k_blk, preferred_element_type=jnp.float32)  37.2 us
    dot_general x32, matrix products, block_terms(): jnp.einsum('hqk,khd->hqd', weights.astype(jnp.bfloat16), v_blk, preferred...  34.5 us
    another operation x1, loops' own time, local(): lax.scan(visit, state, (k_split, v_split, jnp.arange(block_count, dtype=j...  19.5 us
    while x2, local copies, waits for them, and re-layouts, local(): lax.scan(visit, state, (k_split, v_split, jnp.arange(block_count, dtype=j...  19.5 us
    dynamic_slice x32, local copies, waits for them, and re-layouts, local(): lax.scan(visit, state, (k_split, v_split, jnp.arange(block_count, dtype=j...  18.8 us
    all_to_all x1, waiting for transfers between devices, summed_on_arrival(): lax.all_to_all(in_blocks(shard, dim, devices), axis, 0, 0, tiled=True)  15.3 us
  transfers between devices with their start and end apart: 4, of which 3 were waited for; matrix products, arithmetic and copies ran while one was open for 2% of the time, Pallas kernels for 0%

commit v1 on v0

--- a/solution.py
+++ b/solution.py
@@ -143,7 +143,9 @@
     )
     conv_out = jax.nn.silu(normed).astype(jnp.bfloat16)
     q_heads = query.reshape(rows_here, heads_here, head_dim)
-    cum_all = lax.all_gather(cum_gate.T, "sp", axis=0, tiled=True)
+    cum_all = jnp.concatenate(
+        lax.all_to_all(jnp.stack([cum_gate.T] * lax.axis_size("sp")), "sp", 0, 0), axis=0
+    )
     own_first = lax.axis_index("sp") * rows_here
     start_state = (
         jnp.full((heads_here, rows_here), neg_large, jnp.float32),

time: 349 us -> 353 us (1.011)
  blocking collectives: 65.5 us -> 13.1 us
  waiting for transfers between devices: 80.7 us -> 129 us
  starting transfers between devices: 10.5 us -> 14.9 us
    all_gather x1 -> x0, blocking collectives: 53 us -> none  [local(): cum_all = lax.all_gather(cum_gate.T, 'sp', axis=0, tiled=True)]
    all_gather x1, waiting for transfers between devices: 53.7 us -> 98.2 us  [sent_together(): filled, at, outs = (lax.all_gather(both, axis, axis=dim, tiled=True), 0, [])]
    all_to_all x0 -> x1, starting transfers between devices: none -> 5.16 us  [local(): lax.all_to_all(jnp.stack([cum_gate.T] * lax.axis_size('sp')), 'sp', 0, 0)]
    ppermute x1, waiting for transfers between devices: 0.01 us -> 4.08 us  [passed_along(): return lax.ppermute(block, axis, route)]
  transfers between devices with their start and end apart: 4 -> 5, of which waited for: 3 -> 4; matrix products, arithmetic and copies ran while one was open for 2% -> 14% of each run, Pallas kernels for 0% -> 0%
where the time goes in v1:
time: 353 us; the launch traced here: 349 us
  waiting for transfers between devices  129 us (37%)
  matrix products  76.6 us (22%)
  local copies, waits for them, and re-layouts  67.8 us (19%)
  loops' own time  22.9 us (6%)
  starting transfers between devices  14.9 us (4%)
  between operations  14.4 us (4%)
  blocking collectives  13.1 us (4%)
  other arithmetic  10 us (3%)
    all_gather x1, waiting for transfers between devices, sent_together(): filled, at, outs = (lax.all_gather(both, axis, axis=dim, tiled=True), 0, [])  98.2 us
    dot_general x32, matrix products, block_terms(): jnp.einsum('qhd,khd->hqk', q_blk, k_blk, preferred_element_type=jnp.float32)  37.2 us
    dot_general x32, matrix products, block_terms(): jnp.einsum('hqk,khd->hqd', weights.astype(jnp.bfloat16), v_blk, preferred...  34.6 us
    another operation x1, loops' own time, local(): lax.scan(visit, state, (k_split, v_split, jnp.arange(block_count, dtype=j...  21.4 us
    while x2, local copies, waits for them, and re-layouts, local(): lax.scan(visit, state, (k_split, v_split, jnp.arange(block_count, dtype=j...  19.5 us
    dynamic_slice x32, local copies, waits for them, and re-layouts, local(): lax.scan(visit, state, (k_split, v_split, jnp.arange(block_count, dtype=j...  19.3 us
    all_to_all x1, waiting for transfers between devices, summed_on_arrival(): lax.all_to_all(in_blocks(shard, dim, devices), axis, 0, 0, tiled=True)  15.1 us
    psum x1, blocking collectives, local(): lax.psum((jnp.sum(conv_sum, axis=1), jnp.sum(conv_sum * conv_sum, axis=1)...  13.1 us
  transfers between devices with their start and end apart: 5, of which 4 were waited for; matrix products, arithmetic and copies ran while one was open for 14% of the time, Pallas kernels for 0%

profile of v1, /device:TPU:2016, one launch (start us, length us, event | category | flops | bytes accessed | tf_op | source)
XLA Modules:
  0.0 348.7 jit_solution(16665642750519962649)
XLA Ops:
  9.4 4.6 %all-to-all-start = ((bf16[8,256,256]{1,2,0:T(8,128)(2,1)}), bf16[8,256,256]{1,2,0:T(8,128)(2,1)S(1)}, u32[]{:S(2)}, u32[]{:S(2)}) async-start(bf16[8,256,256]{1,2,0:T(8,128)(2,1)} %broadcast_in_dim.25), calls=%async_computation | async-start | bytes 2097152 | tf_op jit(solution)/shard_map/all_to_all | solution.py:13
  18.3 11.6 %all-to-all-done = bf16[8,256,256]{1,2,0:T(8,128)(2,1)S(1)} async-done(((bf16[8,256,256]{1,2,0:T(8,128)(2,1)}), bf16[8,256,256]{1,2,0:T(8,128)(2,1)S(1)}, u32[]{:S(2)}, u32[]{:S(2)}) %all-to-all-start) | async-done | bytes 1048608 | tf_op jit(solution)/shard_map/all_to_all | solution.py:13
  30.6 2.8 fusion.62
  34.8 5.2 %all-to-all-start.1 = ((f32[32,256,2]{1,2,0:T(2,128)}), f32[32,256,2]{1,2,0:T(2,128)S(1)}, u32[]{:S(2)}, u32[]{:S(2)}) async-start(f32[32,256,2]{1,2,0:T(2,128)} %stack.2), calls=%async_computation.1 | async-start | bytes 131072 | tf_op jit(solution)/shard_map/all_to_all | solution.py:147
  41.6 4.1 %collective-permute-done = bf16[30,128]{1,0:T(8,128)(2,1)S(1)} collective-permute-done((bf16[30,128]{1,0:T(8,128)(2,1)S(1)}, bf16[30,128]{1,0:T(8,128)(2,1)S(1)}, u32[]{:S(2)}, u32[]{:S(2)}) %collective-permute-start) | collective-permute-done | bytes 7712 | tf_op jit(solution)/shard_map/ppermute | solution.py:32
  46.3 13.1 %all-reduce = (f32[256]{0:T(256)S(1)}, f32[256]{0:T(256)S(1)}) all-reduce(f32[256]{0:T(256)S(1)} %get-tuple-element.195, f32[256]{0:T(256)S(1)} %get-tuple-element.194), channel_id=1, replica_groups=mesh['grp'=2,'sp'=32,'tp'=8] {'tp'}, use_global_device_ids=true, to_apply=%region_4.0 | all-reduce | flops 512 | bytes 4096 | tf_op jit(solution)/shard_map/psum | solution.py:136
  59.9 98.2 %all-gather.2.cloned.1.call-done = bf16[8192,256]{1,0:T(8,128)(2,1)} async-done(((bf16[256,256]{1,0:T(8,128)(2,1)}), bf16[8192,256]{1,0:T(8,128)(2,1)}) %all-gather.2.cloned.1.call-update) | async-done | bytes 4194320 | tf_op jit(solution)/shard_map/all_gather | solution.py:37
  158.1 4.5 %fusion.61 = (bf16[8192,128]{1,0:T(8,128)(2,1)}, bf16[8192,128]{1,0:T(8,128)(2,1)}) fusion(bf16[8192,256]{1,0:T(8,128)(2,1)} %all-gather.2.cloned.1.call-done), kind=kLoop, calls=%fused_computation.157 | loop fusion | bytes 8388608 | tf_op jit(solution)/shard_map/slice | solution.py:39
  162.6 8.2 %reshape.92 = bf16[32,256,2,64]{3,2,1,0:T(2,128)(2,1)} reshape(bf16[8192,128]{1,0:T(8,128)(2,1)} %get-tuple-element.229) | data formatting | bytes 4194304 | tf_op jit(solution)/shard_map/reshape | solution.py:159
  170.8 9.7 %copy.31 = bf16[32,256,2,64]{1,3,2,0:T(8,128)(2,1)} copy(bf16[32,256,2,64]{3,2,1,0:T(2,128)(2,1)} %reshape.92) | data formatting | bytes 4194304 | tf_op jit(solution)/shard_map/while | solution.py:176
  180.5 8.2 %reshape.91 = bf16[32,256,2,64]{3,2,1,0:T(2,128)(2,1)} reshape(bf16[8192,128]{1,0:T(8,128)(2,1)} %get-tuple-element.230) | data formatting | bytes 4194304 | tf_op jit(solution)/shard_map/reshape | solution.py:158
  188.7 9.7 %copy.30 = bf16[32,256,2,64]{1,3,2,0:T(8,128)(2,1)} copy(bf16[32,256,2,64]{3,2,1,0:T(2,128)(2,1)} %reshape.91) | data formatting | bytes 4194304 | tf_op jit(solution)/shard_map/while | solution.py:176
  198.5 121.5 %while.14 = (s32[]{:T(128)}, f32[2,256]{1,0:T(2,128)S(1)}, f32[2,256]{1,0:T(2,128)S(1)}, f32[2,256,64]{1,2,0:T(8,128)S(1)}, s32[32]{0:T(128)S(1)}, /*index=5*/s3...) while((s32[]{:T(128)}, f32[2,256]{1,0:T(2,128)S(1)}, ...), condition=%wide.region_10.11_spmd, body=%wide.region_5.10_spmd.sunk | while | flops 34966024 | bytes 2205049 | solution.py:176
  199.8 2.5 conditional.2
  203.6 2.5 conditional.2
  207.4 2.5 conditional.2
  218.8 2.5 conditional.2
  222.5 2.5 conditional.2
  233.9 2.5 conditional.2
  237.7 2.5 conditional.2
  249.1 2.5 conditional.2
  264.3 2.5 conditional.2
  321.5 3.8 %all-to-all-start.2 = ((bf16[8,32,2048]{2,1,0:T(8,128)(2,1)}), bf16[8,32,2048]{2,1,0:T(8,128)(2,1)S(1)}, u32[]{:S(2)}, u32[]{:S(2)}) async-start(bf16[8,32,2048]{2,1,0:T(8,128)(2,1)} %bitcast.100), calls=%async_computation.2 | async-start | bytes 2097152 | tf_op jit(solution)/shard_map/all_to_all | solution.py:52
  325.9 15.1 %all-to-all-done.2 = bf16[8,32,2048]{2,1,0:T(8,128)(2,1)S(1)} async-done(((bf16[8,32,2048]{2,1,0:T(8,128)(2,1)}), bf16[8,32,2048]{2,1,0:T(8,128)(2,1)S(1)}, u32[]{:S(2)}, u32[]{:S(2)}) %all-to-all-start.2) | async-done | bytes 1048608 | tf_op jit(solution)/shard_map/all_to_all | solution.py:52
  (337 shorter events, 170.5 us)
Async XLA Ops:
  7.2 52.2 %copy-start = (bf16[128,2048]{1,0:T(8,128)(2,1)S(1)}, bf16[128,2048]{1,0:T(8,128)(2,1)}, u32[]{:S(2)}) copy-start(bf16[128,2048]{1,0:T(8,128)(2,1)} %param.26) | copy-start | bytes 1572868
  7.2 6.9 %copy-start.8 = (bf16[2048]{0:T(1024)(128)(2,1)S(1)}, bf16[2048]{0:T(1024)(128)(2,1)}, u32[]{:S(2)}) copy-start(bf16[2048]{0:T(1024)(128)(2,1)} %param.17) | copy-start | bytes 12292
  7.2 6.9 %copy-start.2 = (bf16[128,2048]{1,0:T(8,128)(2,1)S(1)}, bf16[128,2048]{1,0:T(8,128)(2,1)}, u32[]{:S(2)}) copy-start(bf16[128,2048]{1,0:T(8,128)(2,1)} %param.18) | copy-start | bytes 1572868
  7.2 7.7 %copy-start.3 = (bf16[128,2048]{1,0:T(8,128)(2,1)S(1)}, bf16[128,2048]{1,0:T(8,128)(2,1)}, u32[]{:S(2)}) copy-start(bf16[128,2048]{1,0:T(8,128)(2,1)} %param.19) | copy-start | bytes 1572868
  8.3 7.4 %copy-start.4 = (bf16[128,2048]{1,0:T(8,128)(2,1)S(1)}, bf16[128,2048]{1,0:T(8,128)(2,1)}, u32[]{:S(2)}) copy-start(bf16[128,2048]{1,0:T(8,128)(2,1)} %param.22) | copy-start | bytes 1572868
  9.4 20.5 %all-to-all-start = ((bf16[8,256,256]{1,2,0:T(8,128)(2,1)}), bf16[8,256,256]{1,2,0:T(8,128)(2,1)S(1)}, u32[]{:S(2)}, u32[]{:S(2)}) async-start(bf16[8,256,256]{1,2,0:T(8,128)(2,1)} %broadcast_in_dim.25), calls=%async_computation | async-start | bytes 2097152 | tf_op jit(solution)/shard_map/all_to_all | solution.py:13
  14.0 144.1 %all-gather.2.cloned.1.call-start = ((), (), s32[]{:S(2)}) async-start(), calls=%async_computation.3 | async-start | bytes 4325376 | tf_op jit(solution)/shard_map/all_gather | solution.py:37
  14.1 2.6 copy-start.5
  14.1 3.4 copy-start.6
  30.6 3.6 %copy-start.9 = (f32[2,256]{1,0:T(2,128)S(1)}, f32[2,256]{1,0:T(2,128)}, u32[]{:S(2)}) copy-start(f32[2,256]{1,0:T(2,128)} %param.25) | copy-start | bytes 6148
  30.6 9.4 %copy-start.7 = (bf16[31,128]{1,0:T(8,128)(2,1)S(1)}, bf16[31,128]{1,0:T(8,128)(2,1)}, u32[]{:S(2)}) copy-start(bf16[31,128]{1,0:T(8,128)(2,1)} %param.20) | copy-start | bytes 23812
  30.6 10.8 %copy-start.10 = (bf16[128]{0:T(256)(128)(2,1)S(1)}, bf16[128]{0:T(256)(128)(2,1)}, u32[]{:S(2)}) copy-start(bf16[128]{0:T(256)(128)(2,1)} %param.21) | copy-start | bytes 772
  34.8 163.6 %all-to-all-start.1 = ((f32[32,256,2]{1,2,0:T(2,128)}), f32[32,256,2]{1,2,0:T(2,128)S(1)}, u32[]{:S(2)}, u32[]{:S(2)}) async-start(f32[32,256,2]{1,2,0:T(2,128)} %stack.2), calls=%async_computation.1 | async-start | bytes 131072 | tf_op jit(solution)/shard_map/all_to_all | solution.py:147
  40.1 5.6 %collective-permute-start = (bf16[30,128]{1,0:T(8,128)(2,1)S(1)}, bf16[30,128]{1,0:T(8,128)(2,1)S(1)}, u32[]{:S(2)}, u32[]{:S(2)}) collective-permute-start(bf16[30,128]{1,0:T(8,128)(2,1)S(1)} %slice.282), channel_id=1, source_target_pairs={{0,8},{8,16},{16,24},{24,32},{32,40},{40,48},{48,56},{56,64},{64,7... | collective-permute-start | bytes 23048 | tf_op jit(solution)/shard_map/ppermute | solution.py:32
  198.5 121.6 %copy-start.1 = (bf16[128,2048]{1,0:T(8,128)(2,1)S(1)}, bf16[128,2048]{1,0:T(8,128)(2,1)}, u32[]{:S(2)}) copy-start(bf16[128,2048]{1,0:T(8,128)(2,1)} %param.27) | copy-start | bytes 1572868
  321.5 19.5 %all-to-all-start.2 = ((bf16[8,32,2048]{2,1,0:T(8,128)(2,1)}), bf16[8,32,2048]{2,1,0:T(8,128)(2,1)S(1)}, u32[]{:S(2)}, u32[]{:S(2)}) async-start(bf16[8,32,2048]{2,1,0:T(8,128)(2,1)} %bitcast.100), calls=%async_computation.2 | async-start | bytes 2097152 | tf_op jit(solution)/shard_map/all_to_all | solution.py:52
Sparse Core Ops, SparseCore 0:
  34.3 123.7 all-gather.1
